TPU v7x, 32 devices: a whole 2x2x4 slice. The times are simulated.
32 devices in a mesh: sp: 8 (over z, x), dp: 4 (over y, core).
Axes of the slice: x: 2, y: 2, z: 4, core: 2. Of those that a mesh axis runs over, the one named last changes fastest.
Arguments:
- normed_input: bfloat16 [2560, 2048], P('sp'), may hold values from -6 to 6
- out_grad: bfloat16 [2560, 2048], P('sp'), may hold values from -6 to 6
- value_weight: bfloat16 [2048, 1024], P(None, 'dp'), may hold values from -0.125 to 0.125
- gate_weight: bfloat16 [2048, 1024], P(None, 'dp'), may hold values from -0.125 to 0.125
- down_weight: bfloat16 [1024, 2048], P('dp'), may hold values from -0.1875 to 0.1875
- conv_kernel: float32 [31, 1024], P(None, 'dp'), may hold values from -5 to 5
- conv_bias: float32 [1024], P('dp'), may hold values from -3 to 3
- norm_gain: float32 [1024], P('dp'), may hold values from 0.1 to 1.9
- norm_shift: float32 [1024], P('dp'), may hold values from -3 to 3
Outputs:
- input_grad: bfloat16 [2560, 2048], P('sp')
- value_grad: float32 [2048, 1024], P('sp', 'dp')
- gate_grad: float32 [2048, 1024], P('sp', 'dp')
- down_grad: float32 [1024, 2048], P('dp', 'sp')
- kernel_grad: float32 [31, 1024], P(None, 'dp')
- bias_grad: float32 [1024], P('dp')
- gain_grad: float32 [1024], P('dp')
- shift_grad: float32 [1024], P('dp')
All inputs are finite; a program needn't handle non-finite values.
Results may differ from a plain program's by a relative error of at most 0.006.
Values may be sent and summed in bfloat16 or wider, within the bound.
A program may use at most 64 MiB of HBM per device.

v0:
```python
import math
import jax
import jax.numpy as jnp
from jax import lax
from jax.sharding import PartitionSpec as P

EPS = 1e-05


def with_halo(block, sides, width):
    for axis, dim in sides:
        count = lax.axis_size(axis)
        forward = [(i, i + 1) for i in range(count - 1)]
        backward = [(target, source) for source, target in forward]
        low = lax.ppermute(
            lax.slice_in_dim(block, block.shape[dim] - width, None, axis=dim), axis, forward
        )
        high = lax.ppermute(lax.slice_in_dim(block, 0, width, axis=dim), axis, backward)
        block = jnp.concatenate([low, block, high], axis=dim)
    return block


def project(weight, rows):
    return lax.dot_general(
        weight, rows, (((0,), (1,)), ((), ())), preferred_element_type=jnp.float32
    )


def on_device(
    normed_input,
    out_grad,
    value_weight,
    gate_weight,
    down_weight,
    conv_kernel,
    conv_bias,
    norm_gain,
    norm_shift,
):
    tokens = normed_input.shape[0]
    width = conv_kernel.shape[0]
    reach = width // 2
    local_channels = value_weight.shape[1]
    channels = local_channels * lax.axis_size("dp")
    ratio = 1.0 / math.sqrt(tokens * lax.axis_size("sp"))
    value_b = project(value_weight, normed_input).astype(jnp.bfloat16)
    gate_b = project(gate_weight, normed_input).astype(jnp.bfloat16)
    value = lax.optimization_barrier(value_b).astype(jnp.float32)
    gate = lax.optimization_barrier(gate_b).astype(jnp.float32)
    opening = jax.nn.sigmoid(gate)
    glu = value * opening
    padded = with_halo(glu, (("sp", 1),), reach)
    mixed = jnp.zeros_like(glu) + conv_bias[:, None]
    for tap in range(width):
        mixed = mixed + conv_kernel[tap][:, None] * padded[:, tap : tap + tokens]
    total, squares = lax.psum((jnp.sum(mixed, axis=0), jnp.sum(mixed * mixed, axis=0)), "dp")
    mean = total / channels
    spread = squares / channels - mean * mean
    inv_std = lax.rsqrt(spread + EPS)
    centred = (mixed - mean[None, :]) * inv_std[None, :]
    normed = centred * norm_gain[:, None] + norm_shift[:, None]
    sig = jax.nn.sigmoid(normed)
    activated = (normed * sig).astype(jnp.bfloat16)
    d_act = lax.dot_general(
        down_weight, out_grad, (((1,), (1,)), ((), ())), preferred_element_type=jnp.float32
    )
    d_normed = d_act * sig * (1.0 + normed * (1.0 - sig))
    d_centred = d_normed * norm_gain[:, None]
    first, second = lax.psum(
        (jnp.sum(d_centred, axis=0), jnp.sum(d_centred * centred, axis=0)), "dp"
    )
    d_mixed = inv_std[None, :] * (
        d_centred - first[None, :] / channels - centred * (second[None, :] / channels)
    )
    d_padded = with_halo(d_mixed, (("sp", 1),), reach)
    d_glu = jnp.zeros_like(d_mixed)
    for tap in range(width):
        d_glu = (
            d_glu
            + conv_kernel[tap][:, None] * d_padded[:, 2 * reach - tap : 2 * reach - tap + tokens]
        )
    kernel_local = jnp.stack(
        [jnp.sum(d_mixed * padded[:, tap : tap + tokens], axis=1) for tap in range(width)]
    )
    kernel_grad, bias_grad, gain_grad, shift_grad = lax.psum(
        (
            kernel_local * ratio,
            jnp.sum(d_mixed, axis=1) * ratio,
            jnp.sum(d_normed * centred, axis=1) * ratio,
            jnp.sum(d_normed, axis=1) * ratio,
        ),
        "sp",
    )
    d_value = (d_glu * opening).astype(jnp.bfloat16)
    d_gate = (d_glu * value * opening * (1.0 - opening)).astype(jnp.bfloat16)
    numbers = (((0,), (1,)), ((), ()))
    value_part = lax.dot_general(normed_input, d_value, numbers, preferred_element_type=jnp.float32)
    gate_part = lax.dot_general(normed_input, d_gate, numbers, preferred_element_type=jnp.float32)
    down_part = lax.dot_general(out_grad, activated, numbers, preferred_element_type=jnp.float32)
    summed = lax.psum_scatter(
        jnp.concatenate([value_part, gate_part, down_part], axis=1) * ratio,
        "sp",
        scatter_dimension=0,
        tiled=True,
    )
    value_grad = summed[:, :local_channels]
    gate_grad = summed[:, local_channels : 2 * local_channels]
    down_grad = summed[:, 2 * local_channels :].T
    numbers = (((0,), (1,)), ((), ()))
    own = lax.dot_general(d_value, value_weight, numbers, preferred_element_type=jnp.float32)
    own = own + lax.dot_general(d_gate, gate_weight, numbers, preferred_element_type=jnp.float32)
    input_grad = lax.psum(own, "dp").astype(jnp.bfloat16)
    return (
        input_grad,
        value_grad,
        gate_grad,
        down_grad,
        kernel_grad,
        bias_grad,
        gain_grad,
        shift_grad,
    )


def solution(mesh):
    in_specs = (
        P("sp", None),
        P("sp", None),
        P(None, "dp"),
        P(None, "dp"),
        P("dp", None),
        P(None, "dp"),
        P("dp"),
        P("dp"),
        P("dp"),
    )
    out_specs = (
        P("sp", None),
        P("sp", "dp"),
        P("sp", "dp"),
        P("dp", "sp"),
        P(None, "dp"),
        P("dp"),
        P("dp"),
        P("dp"),
    )
    return jax.shard_map(
        on_device, mesh=mesh, in_specs=in_specs, out_specs=out_specs, check_vma=False
    )
```

profile of v0, /device:TPU:0, one launch (start us, length us, event | category | flops | bytes accessed | tf_op | source)
XLA Modules:
  0.0 185.2 jit_solution(6150821379646648669)
XLA Ops:
  7.2 0.0 copy-start
  7.2 0.0 copy-start.1
  7.2 0.0 reduce-scatter.2.cloned.1.call-start
  7.2 1.2 copy-done
  8.5 1.7 convolution_convert_fusion.1
  10.2 0.0 copy-done.1
  10.2 0.0 copy-start.3
  10.2 0.0 copy-start.5
  10.3 0.0 copy-start.4
  10.3 0.0 copy-start.6
  10.3 0.5 convolution_convert_fusion
  10.8 0.1 convert_multiply_fusion.1
  10.9 4.9 %collective-permute-start = (f32[256,15]{0,1:T(8,128)S(1)}, f32[256,15]{0,1:T(8,128)S(1)}, u32[]{:S(2)}, u32[]{:S(2)}) collective-permute-start(f32[256,15]{0,1:T(8,128)S(1)} %get-tuple-element.71), channel_id=1, source_target_pairs={{0,4},{4,8},{8,12},{12,16},{16,20},{20,24},{24,28},{1,5},{5,9},{9,... | collective-permute-start | bytes 46088 | tf_op jit(solution)/shard_map/ppermute | solution.py:15
  15.8 1.3 collective-permute-start.1
  17.1 0.0 copy-done.3
  17.2 0.1 collective-permute-done
  17.2 4.2 %collective-permute-done.1 = f32[256,15]{0,1:T(8,128)S(1)} collective-permute-done((f32[256,15]{0,1:T(8,128)S(1)}, f32[256,15]{0,1:T(8,128)S(1)}, u32[]{:S(2)}, u32[]{:S(2)}) %collective-permute-start.1) | collective-permute-done | bytes 15392 | tf_op jit(solution)/shard_map/ppermute | solution.py:18
  21.4 0.0 copy-done.5
  21.4 1.7 multiply_reduce_fusion.33
  23.2 5.7 %all-reduce.2 = (f32[320]{0:T(512)S(1)}, f32[320]{0:T(512)S(1)}) all-reduce(f32[320]{0:T(512)S(1)} %get-tuple-element.53, f32[320]{0:T(512)S(1)} %get-tuple-element.52), channel_id=1, replica_groups=mesh['sp'=8,'dp'=4] {'dp'}, use_global_device_ids=true, to_apply=%region_3.0 | all-reduce | flops 640 | bytes 5120 | tf_op jit(solution)/shard_map/psum | solution.py:56
  28.8 0.0 copy-done.4
  28.8 0.0 copy-done.6
  28.8 2.4 %multiply_reduce_fusion = (f32[256]{0:T(256)S(1)}, f32[320]{0:T(512)S(1)}, f32[320]{0:T(512)S(1)}, f32[256]{0:T(256)S(1)}, f32[256,320]{0,1:T(8,128)S(1)}) fusion(f32[256,320]{0,1:T(8,128)S(1)} %get-tuple-element.65, f32[320]{0:T(512)S(1)} %get-tuple-element.105, f32[320]{0:T(512)S(1)} %get-tuple-element.104, f32[256]{0:T(256)S(1)} %copy-done.4, ...), kind=kOutput, calls=%fused_computation.214 | convolution fusion | flops 337099648 | bytes 3023872 | tf_op jit(solution)/shard_map/dot_general | solution.py:64
  31.2 6.6 %all-reduce.1 = (f32[320]{0:T(512)S(1)}, f32[320]{0:T(512)S(1)}) all-reduce(f32[320]{0:T(512)S(1)} %get-tuple-element.47, f32[320]{0:T(512)S(1)} %get-tuple-element.48), channel_id=1, replica_groups=mesh['sp'=8,'dp'=4] {'dp'}, use_global_device_ids=true, to_apply=%region_7.0 | all-reduce | flops 640 | bytes 5120 | tf_op jit(solution)/shard_map/psum | solution.py:69
  37.9 0.5 multiply_reduce_fusion.1
  38.4 1.3 collective-permute-start.2
  39.7 5.0 %collective-permute-start.3 = (f32[256,15]{0,1:T(8,128)S(1)}, f32[256,15]{0,1:T(8,128)S(1)}, u32[]{:S(2)}, u32[]{:S(2)}) collective-permute-start(f32[256,15]{0,1:T(8,128)S(1)} %get-tuple-element.70), channel_id=1, source_target_pairs={{0,4},{4,8},{8,12},{12,16},{16,20},{20,24},{24,28},{1,5},{5,9},{9,... | collective-permute-start | bytes 46088 | tf_op jit(solution)/shard_map/ppermute | solution.py:15
  44.7 2.2 %convolution_bitcast_fusion = f32[2048,256]{0,1:T(8,128)S(1)} fusion(bf16[320,2048]{1,0:T(8,128)(2,1)} %param.10, f32[256,320]{0,1:T(8,128)S(1)} %get-tuple-element.65, f32[256]{0:T(256)S(1)} %copy-done.6, f32[256]{0:T(256)S(1)} %copy-done.4, f32[320]{0:T(512)S(1)} %get-tuple-element.105, f32[320]{0:T(512)S(1)} %get-tuple-element.104), kind=kOutput, calls=%fused_computation.2 | convolution fusion | flops 336281600 | bytes 3740160 | tf_op jit(solution)/shard_map/dot_general | solution.py:99
  46.9 0.0 collective-permute-done.2
  46.9 0.0 collective-permute-done.3
  46.9 1.7 fusion.3
  48.6 0.7 convolution_bitcast_fusion.1
  49.3 0.8 convolution_bitcast_fusion.2
  50.1 3.3 %maximum_multiply_fusion = f32[2048,768]{0,1:T(8,128)} fusion(f32[2048,256]{0,1:T(8,128)S(1)} %convolution_bitcast_fusion, f32[2048,256]{0,1:T(8,128)S(1)} %convolution_bitcast_fusion.1, f32[2048,256]{0,1:T(8,128)S(1)} %convolution_bitcast_fusion.2), kind=kLoop, calls=%fused_computation | loop fusion | flops 4718592 | bytes 12582912 | tf_op jit(solution)/shard_map/mul | solution.py:101
  53.4 0.0 reduce-scatter.2.cloned.1.call-update
  53.4 0.3 multiply_reduce_fusion.26
  53.7 0.4 multiply_reduce_fusion.17
  54.1 0.4 multiply_reduce_fusion.10
  54.5 0.1 stack.127
  54.6 0.0 copy-start.2
  54.6 40.4 %all-reduce = (f32[31,256]{1,0:T(8,128)}, f32[256]{0:T(256)}, f32[256]{0:T(256)}, f32[256]{0:T(256)}) all-reduce(f32[31,256]{1,0:T(8,128)S(1)} %broadcast_multiply_fusion, f32[256]{0:T(256)S(1)} %broadcast_multiply_fusion.6, f32[256]{0:T(256)S(1)} %get-tuple-element.108, ...), channel_id=1, replica_groups=mesh['sp'=8,'dp'=4] {'sp'}, use_global_device_ids=true, to_apply=%region_41.0 | all-reduce | flops 8704 | bytes 69632 | tf_op jit(solution)/shard_map/psum | solution.py:85
  95.0 1.8 fusion.126
  96.8 0.0 copy-done.2
  96.8 2.1 %convolution_add_fusion = f32[320,2048]{1,0:T(8,128)} fusion(f32[320,2048]{1,0:T(8,128)S(1)} %fusion.126, bf16[256,320]{0,1:T(8,128)(2,1)S(1)} %get-tuple-element.63, bf16[2048,256]{1,0:T(8,128)(2,1)S(1)} %copy-done.2), kind=kOutput, calls=%fused_computation.1 | convolution fusion | flops 336199680 | bytes 6455296 | tf_op jit(solution)/shard_map/dot_general | solution.py:111
  98.9 50.2 %all-reduce.4 = bf16[320,2048]{1,0:T(8,128)(2,1)} all-reduce(f32[320,2048]{1,0:T(8,128)} %convolution_add_fusion), channel_id=1, replica_groups=mesh['sp'=8,'dp'=4] {'dp'}, use_global_device_ids=true, to_apply=%region_8.0 | all-reduce | flops 655360 | bytes 3932160 | tf_op jit(solution)/shard_map/psum | solution.py:112
  149.1 25.7 %reduce-scatter.2.cloned.1.call-done = f32[256,768]{0,1:T(8,128)} async-done(((f32[2048,768]{0,1:T(8,128)}), f32[256,768]{0,1:T(8,128)}) %reduce-scatter.2.cloned.1.call-update) | async-done | bytes 786448 | tf_op jit(solution)/shard_map/reduce_scatter | solution.py:100
  174.8 1.9 %slice_bitcast_fusion = (f32[256,256]{1,0:T(8,128)}, f32[256,256]{0,1:T(8,128)S(1)}, f32[256,256]{0,1:T(8,128)S(1)}) fusion(f32[256,768]{0,1:T(8,128)} %reduce-scatter.2.cloned.1.call-done), kind=kLoop, calls=%fused_computation.257 | loop fusion | bytes 1572864 | tf_op jit(solution)/shard_map/transpose | solution.py:108
  176.6 0.8 copy.18
  177.5 0.8 copy.17
  (9 shorter events, 0.1 us)
Async XLA Ops:
  7.2 1.3 copy-start
  7.2 3.0 %copy-start.1 = (bf16[2048,256]{1,0:T(8,128)(2,1)S(1)}, bf16[2048,256]{1,0:T(8,128)(2,1)}, u32[]{:S(2)}) copy-start(bf16[2048,256]{1,0:T(8,128)(2,1)} %param.12) | copy-start | bytes 3145732
  7.2 167.6 %reduce-scatter.2.cloned.1.call-start = ((), (), s32[]{:S(2)}) async-start(), calls=%async_computation.1 | async-start | bytes 7077888 | tf_op jit(solution)/shard_map/reduce_scatter | solution.py:100
  10.2 6.9 %copy-start.3 = (f32[31,256]{1,0:T(8,128)S(1)}, f32[31,256]{1,0:T(8,128)}, u32[]{:S(2)}) copy-start(f32[31,256]{1,0:T(8,128)} %param.14) | copy-start | bytes 95236
  10.2 11.2 %copy-start.5 = (f32[256]{0:T(256)S(1)}, f32[256]{0:T(256)}, u32[]{:S(2)}) copy-start(f32[256]{0:T(256)} %param.15) | copy-start | bytes 3076
  10.3 18.6 %copy-start.4 = (f32[256]{0:T(256)S(1)}, f32[256]{0:T(256)}, u32[]{:S(2)}) copy-start(f32[256]{0:T(256)} %param.16) | copy-start | bytes 3076
  10.3 18.6 %copy-start.6 = (f32[256]{0:T(256)S(1)}, f32[256]{0:T(256)}, u32[]{:S(2)}) copy-start(f32[256]{0:T(256)} %param.17) | copy-start | bytes 3076
  10.9 6.3 %collective-permute-start = (f32[256,15]{0,1:T(8,128)S(1)}, f32[256,15]{0,1:T(8,128)S(1)}, u32[]{:S(2)}, u32[]{:S(2)}) collective-permute-start(f32[256,15]{0,1:T(8,128)S(1)} %get-tuple-element.71), channel_id=1, source_target_pairs={{0,4},{4,8},{8,12},{12,16},{16,20},{20,24},{24,28},{1,5},{5,9},{9,... | collective-permute-start | bytes 46088 | tf_op jit(solution)/shard_map/ppermute | solution.py:15
  15.8 5.6 %collective-permute-start.1 = (f32[256,15]{0,1:T(8,128)S(1)}, f32[256,15]{0,1:T(8,128)S(1)}, u32[]{:S(2)}, u32[]{:S(2)}) collective-permute-start(f32[256,15]{0,1:T(8,128)S(1)} %get-tuple-element.72), channel_id=1, source_target_pairs={{4,0},{8,4},{12,8},{16,12},{20,16},{24,20},{28,24},{5,1},{9,5},{13... | collective-permute-start | bytes 46088 | tf_op jit(solution)/shard_map/ppermute | solution.py:18
  38.4 8.5 %collective-permute-start.2 = (f32[256,15]{0,1:T(8,128)S(1)}, f32[256,15]{0,1:T(8,128)S(1)}, u32[]{:S(2)}, u32[]{:S(2)}) collective-permute-start(f32[256,15]{0,1:T(8,128)S(1)} %get-tuple-element.69), channel_id=1, source_target_pairs={{4,0},{8,4},{12,8},{16,12},{20,16},{24,20},{28,24},{5,1},{9,5},{13... | collective-permute-start | bytes 46088 | tf_op jit(solution)/shard_map/ppermute | solution.py:18
  39.7 7.2 %collective-permute-start.3 = (f32[256,15]{0,1:T(8,128)S(1)}, f32[256,15]{0,1:T(8,128)S(1)}, u32[]{:S(2)}, u32[]{:S(2)}) collective-permute-start(f32[256,15]{0,1:T(8,128)S(1)} %get-tuple-element.70), channel_id=1, source_target_pairs={{0,4},{4,8},{8,12},{12,16},{16,20},{20,24},{24,28},{1,5},{5,9},{9,... | collective-permute-start | bytes 46088 | tf_op jit(solution)/shard_map/ppermute | solution.py:15
  54.6 42.2 %copy-start.2 = (bf16[2048,256]{1,0:T(8,128)(2,1)S(1)}, bf16[2048,256]{1,0:T(8,128)(2,1)}, u32[]{:S(2)}) copy-start(bf16[2048,256]{1,0:T(8,128)(2,1)} %param.12) | copy-start | bytes 3145732
Sparse Core Ops, SparseCore 0:
  53.5 121.1 reduce-scatter.1
where the time goes:
time: 186 us; the launch traced here: 185 us
  blocking collectives  103 us (55%)
  waiting for transfers between devices  30 us (16%)
  between operations  14.3 us (8%)
  starting transfers between devices  12.5 us (7%)
  matrix products  12.2 us (7%)
  other arithmetic  8.41 us (5%)
  local copies, waits for them, and re-layouts  4.97 us (3%)
    psum x1, blocking collectives, on_device(): input_grad = lax.psum(own, 'dp').astype(jnp.bfloat16)  50.2 us
    psum x1, blocking collectives, on_device(): lax.psum((kernel_local * ratio, jnp.sum(d_mixed, axis=1) * ratio, jnp.sum...  40.4 us
    reduce_scatter x1, waiting for transfers between devices, on_device(): lax.psum_scatter(jnp.concatenate([value_part, gate_part, down_part], axis...  25.7 us
    ppermute x2, starting transfers between devices, with_halo(): lax.ppermute(lax.slice_in_dim(block, block.shape[dim] - width, None, axis...  9.85 us
    psum x1, blocking collectives, on_device(): lax.psum((jnp.sum(d_centred, axis=0), jnp.sum(d_centred * centred, axis=0...  6.65 us
    psum x1, blocking collectives, on_device(): lax.psum((jnp.sum(mixed, axis=0), jnp.sum(mixed * mixed, axis=0)), 'dp')  5.67 us
    ppermute x2, waiting for transfers between devices, with_halo(): lax.ppermute(lax.slice_in_dim(block, 0, width, axis=dim), axis, backward)  4.21 us
  transfers between devices with their start and end apart: 5, of which 3 were waited for; matrix products, arithmetic and copies ran while one was open for 4% of the time, Pallas kernels for 0%

commit v1 on v0

--- a/solution.py
+++ b/solution.py
@@ -109,7 +109,7 @@
     numbers = (((0,), (1,)), ((), ()))
     own = lax.dot_general(d_value, value_weight, numbers, preferred_element_type=jnp.float32)
     own = own + lax.dot_general(d_gate, gate_weight, numbers, preferred_element_type=jnp.float32)
-    input_grad = lax.psum(own, "dp").astype(jnp.bfloat16)
+    input_grad = jnp.sum(lax.all_gather(own, "dp"), axis=0).astype(jnp.bfloat16)
     return (
         input_grad,
         value_grad,

time: 186 us -> 194 us (1.043)
  waiting for transfers between devices: 30 us -> 80 us
  blocking collectives: 103 us -> 53.1 us
  other arithmetic: 8.41 us -> 14.9 us
    psum x1 -> x0, blocking collectives: 50.2 us -> none  [on_device(): input_grad = lax.psum(own, 'dp').astype(jnp.bfloat16)]
    reduce_scatter x1, waiting for transfers between devices: 25.7 us -> 75.7 us  [on_device(): lax.psum_scatter(jnp.concatenate([value_part, gate_part, down_part], axis...]
    reduce_sum x0 -> x1, other arithmetic: none -> 6.54 us  [on_device(): input_grad = jnp.sum(lax.all_gather(own, 'dp'), axis=0).astype(jnp.bfloat16)]
  transfers between devices with their start and end apart: 5 -> 6, of which waited for: 3 -> 3; matrix products, arithmetic and copies ran while one was open for 4% -> 6% of each run, Pallas kernels for 0% -> 0%
where the time goes in v1:
time: 194 us; the launch traced here: 193 us
  waiting for transfers between devices  80 us (41%)
  blocking collectives  53.1 us (27%)
  between operations  15.7 us (8%)
  other arithmetic  14.9 us (8%)
  starting transfers between devices  12.5 us (6%)
  matrix products  12.2 us (6%)
  local copies, waits for them, and re-layouts  4.97 us (3%)
    reduce_scatter x1, waiting for transfers between devices, on_device(): lax.psum_scatter(jnp.concatenate([value_part, gate_part, down_part], axis...  75.7 us
    psum x1, blocking collectives, on_device(): lax.psum((kernel_local * ratio, jnp.sum(d_mixed, axis=1) * ratio, jnp.sum...  40.8 us
    ppermute x2, starting transfers between devices, with_halo(): lax.ppermute(lax.slice_in_dim(block, block.shape[dim] - width, None, axis...  9.86 us
    psum x1, blocking collectives, on_device(): lax.psum((jnp.sum(d_centred, axis=0), jnp.sum(d_centred * centred, axis=0...  6.65 us
    reduce_sum x1, other arithmetic, on_device(): input_grad = jnp.sum(lax.all_gather(own, 'dp'), axis=0).astype(jnp.bfloat16)  6.54 us
    psum x1, blocking collectives, on_device(): lax.psum((jnp.sum(mixed, axis=0), jnp.sum(mixed * mixed, axis=0)), 'dp')  5.67 us
    ppermute x2, waiting for transfers between devices, with_halo(): lax.ppermute(lax.slice_in_dim(block, 0, width, axis=dim), axis, backward)  4.21 us
  transfers between devices with their start and end apart: 6, of which 3 were waited for; matrix products, arithmetic and copies ran while one was open for 6% of the time, Pallas kernels for 0%

profile of v1, /device:TPU:0, one launch (start us, length us, event | category | flops | bytes accessed | tf_op | source)
XLA Modules:
  0.0 193.4 jit_solution(15434672136551521440)
XLA Ops:
  8.0 0.0 copy-start
  8.0 0.0 copy-start.1
  8.0 0.0 reduce-scatter.2.cloned.1.call-start
  8.1 1.2 copy-done
  9.3 1.7 convolution_convert_fusion.1
  11.1 0.0 copy-done.1
  11.1 0.0 copy-start.3
  11.1 0.0 copy-start.5
  11.1 0.0 copy-start.4
  11.1 0.0 copy-start.6
  11.1 0.5 convolution_convert_fusion
  11.6 0.1 convert_multiply_fusion.1
  11.7 4.9 %collective-permute-start = (f32[256,15]{0,1:T(8,128)S(1)}, f32[256,15]{0,1:T(8,128)S(1)}, u32[]{:S(2)}, u32[]{:S(2)}) collective-permute-start(f32[256,15]{0,1:T(8,128)S(1)} %get-tuple-element.71), channel_id=1, source_target_pairs={{0,4},{4,8},{8,12},{12,16},{16,20},{20,24},{24,28},{1,5},{5,9},{9,... | collective-permute-start | bytes 46088 | tf_op jit(solution)/shard_map/ppermute | solution.py:15
  16.6 1.3 collective-permute-start.1
  17.9 0.0 copy-done.3
  18.0 0.1 collective-permute-done
  18.1 4.2 %collective-permute-done.1 = f32[256,15]{0,1:T(8,128)S(1)} collective-permute-done((f32[256,15]{0,1:T(8,128)S(1)}, f32[256,15]{0,1:T(8,128)S(1)}, u32[]{:S(2)}, u32[]{:S(2)}) %collective-permute-start.1) | collective-permute-done | bytes 15392 | tf_op jit(solution)/shard_map/ppermute | solution.py:18
  22.3 0.0 copy-done.5
  22.3 1.7 multiply_reduce_fusion.33
  24.0 5.7 %all-reduce.2 = (f32[320]{0:T(512)S(1)}, f32[320]{0:T(512)S(1)}) all-reduce(f32[320]{0:T(512)S(1)} %get-tuple-element.53, f32[320]{0:T(512)S(1)} %get-tuple-element.52), channel_id=1, replica_groups=mesh['sp'=8,'dp'=4] {'dp'}, use_global_device_ids=true, to_apply=%region_3.0 | all-reduce | flops 640 | bytes 5120 | tf_op jit(solution)/shard_map/psum | solution.py:56
  29.7 0.0 copy-done.4
  29.7 0.0 copy-done.6
  29.7 2.4 %multiply_reduce_fusion = (f32[256]{0:T(256)S(1)}, f32[320]{0:T(512)S(1)}, f32[320]{0:T(512)S(1)}, f32[256]{0:T(256)S(1)}, f32[256,320]{0,1:T(8,128)S(1)}) fusion(f32[256,320]{0,1:T(8,128)S(1)} %get-tuple-element.65, f32[320]{0:T(512)S(1)} %get-tuple-element.105, f32[320]{0:T(512)S(1)} %get-tuple-element.104, f32[256]{0:T(256)S(1)} %copy-done.4, ...), kind=kOutput, calls=%fused_computation.214 | convolution fusion | flops 337099648 | bytes 3023872 | tf_op jit(solution)/shard_map/dot_general | solution.py:64
  32.0 6.7 %all-reduce.1 = (f32[320]{0:T(512)S(1)}, f32[320]{0:T(512)S(1)}) all-reduce(f32[320]{0:T(512)S(1)} %get-tuple-element.47, f32[320]{0:T(512)S(1)} %get-tuple-element.48), channel_id=1, replica_groups=mesh['sp'=8,'dp'=4] {'dp'}, use_global_device_ids=true, to_apply=%region_7.0 | all-reduce | flops 640 | bytes 5120 | tf_op jit(solution)/shard_map/psum | solution.py:69
  38.7 0.5 multiply_reduce_fusion.1
  39.2 1.3 collective-permute-start.2
  40.5 5.0 %collective-permute-start.3 = (f32[256,15]{0,1:T(8,128)S(1)}, f32[256,15]{0,1:T(8,128)S(1)}, u32[]{:S(2)}, u32[]{:S(2)}) collective-permute-start(f32[256,15]{0,1:T(8,128)S(1)} %get-tuple-element.70), channel_id=1, source_target_pairs={{0,4},{4,8},{8,12},{12,16},{16,20},{20,24},{24,28},{1,5},{5,9},{9,... | collective-permute-start | bytes 46088 | tf_op jit(solution)/shard_map/ppermute | solution.py:15
  45.5 2.2 %convolution_bitcast_fusion = f32[2048,256]{0,1:T(8,128)S(1)} fusion(bf16[320,2048]{1,0:T(8,128)(2,1)} %param.10, f32[256,320]{0,1:T(8,128)S(1)} %get-tuple-element.65, f32[256]{0:T(256)S(1)} %copy-done.6, f32[256]{0:T(256)S(1)} %copy-done.4, f32[320]{0:T(512)S(1)} %get-tuple-element.105, f32[320]{0:T(512)S(1)} %get-tuple-element.104), kind=kOutput, calls=%fused_computation.2 | convolution fusion | flops 336281600 | bytes 3740160 | tf_op jit(solution)/shard_map/dot_general | solution.py:99
  47.7 0.0 collective-permute-done.2
  47.7 0.0 collective-permute-done.3
  47.7 1.7 fusion.3
  49.5 0.7 convolution_bitcast_fusion.1
  50.2 0.8 convolution_bitcast_fusion.2
  50.9 3.3 %maximum_multiply_fusion = f32[2048,768]{0,1:T(8,128)} fusion(f32[2048,256]{0,1:T(8,128)S(1)} %convolution_bitcast_fusion, f32[2048,256]{0,1:T(8,128)S(1)} %convolution_bitcast_fusion.1, f32[2048,256]{0,1:T(8,128)S(1)} %convolution_bitcast_fusion.2), kind=kLoop, calls=%fused_computation | loop fusion | flops 4718592 | bytes 12582912 | tf_op jit(solution)/shard_map/mul | solution.py:101
  54.2 0.0 reduce-scatter.2.cloned.1.call-update
  54.2 0.0 all-gather.3.cloned.1.call-start
  54.3 0.0 copy-start.2
  54.3 1.9 fusion.126
  56.1 0.0 copy-done.2
  56.2 2.1 %convolution_add_fusion = f32[320,2048]{1,0:T(8,128)} fusion(f32[320,2048]{1,0:T(8,128)S(1)} %fusion.126, bf16[256,320]{0,1:T(8,128)(2,1)S(1)} %get-tuple-element.63, bf16[2048,256]{1,0:T(8,128)(2,1)S(1)} %copy-done.2), kind=kOutput, calls=%fused_computation.1 | convolution fusion | flops 336199680 | bytes 6455296 | tf_op jit(solution)/shard_map/dot_general | solution.py:111
  58.2 0.0 all-gather.3.cloned.1.call-update
  58.2 0.3 multiply_reduce_fusion.26
  58.5 0.4 multiply_reduce_fusion.17
  58.9 0.4 multiply_reduce_fusion.10
  59.3 0.1 stack.127
  59.4 40.8 %all-reduce = (f32[31,256]{1,0:T(8,128)}, f32[256]{0:T(256)}, f32[256]{0:T(256)}, f32[256]{0:T(256)}) all-reduce(f32[31,256]{1,0:T(8,128)S(1)} %broadcast_multiply_fusion, f32[256]{0:T(256)S(1)} %broadcast_multiply_fusion.6, f32[256]{0:T(256)S(1)} %get-tuple-element.108, ...), channel_id=1, replica_groups=mesh['sp'=8,'dp'=4] {'sp'}, use_global_device_ids=true, to_apply=%region_41.0 | all-reduce | flops 8704 | bytes 69632 | tf_op jit(solution)/shard_map/psum | solution.py:85
  100.2 75.7 %reduce-scatter.2.cloned.1.call-done = f32[256,768]{0,1:T(8,128)} async-done(((f32[2048,768]{0,1:T(8,128)}), f32[256,768]{0,1:T(8,128)}) %reduce-scatter.2.cloned.1.call-update) | async-done | bytes 786448 | tf_op jit(solution)/shard_map/reduce_scatter | solution.py:100
  175.9 1.9 slice_bitcast_fusion
  177.8 0.8 copy.18
  178.6 0.8 copy.17
  179.4 0.0 all-gather.3.cloned.1.call-done
  179.4 6.5 %reduce_sum.355 = bf16[320,2048]{1,0:T(8,128)(2,1)} reduce(f32[4,320,2048]{2,1,0:T(8,128)} %bitcast.84, f32[]{:T(128)} %constant.6.clone.1), dimensions={0}, to_apply=%region_8.0 | reduce | flops 1966080 | bytes 11796484 | tf_op jit(solution)/shard_map/reduce_sum | solution.py:112
  (9 shorter events, 0.1 us)
Async XLA Ops:
  8.0 1.3 copy-start
  8.0 3.0 %copy-start.1 = (bf16[2048,256]{1,0:T(8,128)(2,1)S(1)}, bf16[2048,256]{1,0:T(8,128)(2,1)}, u32[]{:S(2)}) copy-start(bf16[2048,256]{1,0:T(8,128)(2,1)} %param.12) | copy-start | bytes 3145732
  8.0 167.9 %reduce-scatter.2.cloned.1.call-start = ((), (), s32[]{:S(2)}) async-start(), calls=%async_computation.1 | async-start | bytes 7077888 | tf_op jit(solution)/shard_map/reduce_scatter | solution.py:100
  11.1 6.9 %copy-start.3 = (f32[31,256]{1,0:T(8,128)S(1)}, f32[31,256]{1,0:T(8,128)}, u32[]{:S(2)}) copy-start(f32[31,256]{1,0:T(8,128)} %param.14) | copy-start | bytes 95236
  11.1 11.2 %copy-start.5 = (f32[256]{0:T(256)S(1)}, f32[256]{0:T(256)}, u32[]{:S(2)}) copy-start(f32[256]{0:T(256)} %param.15) | copy-start | bytes 3076
  11.1 18.6 %copy-start.4 = (f32[256]{0:T(256)S(1)}, f32[256]{0:T(256)}, u32[]{:S(2)}) copy-start(f32[256]{0:T(256)} %param.16) | copy-start | bytes 3076
  11.1 18.6 %copy-start.6 = (f32[256]{0:T(256)S(1)}, f32[256]{0:T(256)}, u32[]{:S(2)}) copy-start(f32[256]{0:T(256)} %param.17) | copy-start | bytes 3076
  11.7 6.3 %collective-permute-start = (f32[256,15]{0,1:T(8,128)S(1)}, f32[256,15]{0,1:T(8,128)S(1)}, u32[]{:S(2)}, u32[]{:S(2)}) collective-permute-start(f32[256,15]{0,1:T(8,128)S(1)} %get-tuple-element.71), channel_id=1, source_target_pairs={{0,4},{4,8},{8,12},{12,16},{16,20},{20,24},{24,28},{1,5},{5,9},{9,... | collective-permute-start | bytes 46088 | tf_op jit(solution)/shard_map/ppermute | solution.py:15
  16.6 5.6 %collective-permute-start.1 = (f32[256,15]{0,1:T(8,128)S(1)}, f32[256,15]{0,1:T(8,128)S(1)}, u32[]{:S(2)}, u32[]{:S(2)}) collective-permute-start(f32[256,15]{0,1:T(8,128)S(1)} %get-tuple-element.72), channel_id=1, source_target_pairs={{4,0},{8,4},{12,8},{16,12},{20,16},{24,20},{28,24},{5,1},{9,5},{13... | collective-permute-start | bytes 46088 | tf_op jit(solution)/shard_map/ppermute | solution.py:18
  39.2 8.5 %collective-permute-start.2 = (f32[256,15]{0,1:T(8,128)S(1)}, f32[256,15]{0,1:T(8,128)S(1)}, u32[]{:S(2)}, u32[]{:S(2)}) collective-permute-start(f32[256,15]{0,1:T(8,128)S(1)} %get-tuple-element.69), channel_id=1, source_target_pairs={{4,0},{8,4},{12,8},{16,12},{20,16},{24,20},{28,24},{5,1},{9,5},{13... | collective-permute-start | bytes 46088 | tf_op jit(solution)/shard_map/ppermute | solution.py:18
  40.5 7.2 %collective-permute-start.3 = (f32[256,15]{0,1:T(8,128)S(1)}, f32[256,15]{0,1:T(8,128)S(1)}, u32[]{:S(2)}, u32[]{:S(2)}) collective-permute-start(f32[256,15]{0,1:T(8,128)S(1)} %get-tuple-element.70), channel_id=1, source_target_pairs={{0,4},{4,8},{8,12},{12,16},{16,20},{20,24},{24,28},{1,5},{5,9},{9,... | collective-permute-start | bytes 46088 | tf_op jit(solution)/shard_map/ppermute | solution.py:15
  54.2 125.2 %all-gather.3.cloned.1.call-start = ((), (), s32[]{:S(2)}) async-start(), calls=%async_computation.2 | async-start | bytes 13107200 | tf_op jit(solution)/shard_map/all_gather | solution.py:112
  54.3 1.9 copy-start.2
Sparse Core Ops, SparseCore 0:
  54.3 121.5 reduce-scatter.1
Sparse Core Ops, SparseCore 1:
  58.3 71.9 all-gather.2
